TPU v7x, 32 devices: a whole 2x2x4 slice. The times are simulated.
32 devices in a mesh: fs: 8 (over z, y), tp: 4 (over x, core).
Axes of the slice: x: 2, y: 2, z: 4, core: 2. Of those that a mesh axis runs over, the one named last changes fastest.
Arguments:
- inputs: bfloat16 [16384, 2048], P('fs'), may hold values from -6 to 6
- cotangents: bfloat16 [3, 16384, 1024], P(None, 'fs', 'tp'), as said below
- factor: bfloat16 [2048, 256], P('fs'), as said below
- weights: float32 [3, 2048, 1024], P(None, 'fs', 'tp'), may hold values from -0.125 to 0.125
- first_moment: float32 [3, 256, 1024], P(None, 'fs', 'tp'), may hold values from -0.6 to 0.6
- second_moment: float32 [3, 256, 1024], P(None, 'fs', 'tp'), may hold values from 0.001 to 0.01
Outputs:
- update: float32 [3, 2048, 1024], P(None, 'fs', 'tp')
- new_weights: float32 [3, 2048, 1024], P(None, 'fs', 'tp')
- copies: bfloat16 [3, 2048, 1024], P(None, None, 'tp')
- new_first: float32 [3, 256, 1024], P(None, 'fs', 'tp')
- new_second: float32 [3, 256, 1024], P(None, 'fs', 'tp')
Inputs may be any that keep to these rules, and one draw needn't show every extreme that they name: A real-valued factor of full rank. real-valued cotangents.
All inputs are finite; a program needn't handle non-finite values.
Results may differ from a plain program's by a relative error of at most 0.0085.
Values may be sent and summed in bfloat16 or wider, within the bound.
A program may use at most 64 MiB of HBM per device.

v0:
```python
import jax
import jax.numpy as jnp
from jax import lax
from jax.sharding import PartitionSpec as P

MW = 1024
RANK = 256


def on_device(inputs, cotangents, factor, weights, first_moment, second_moment):
    factor_wide = factor.astype(jnp.float32)
    local_gradient = jnp.einsum(
        "td,mtc->dmc", inputs, cotangents, preferred_element_type=jnp.float32
    )
    gradient_high = local_gradient.astype(jnp.bfloat16)
    gradient_low = (local_gradient - gradient_high.astype(jnp.float32)).astype(jnp.bfloat16)
    factor_piece = lax.all_gather(factor, "fs", axis=0, tiled=True)
    high_term = jnp.einsum(
        "dr,dmc->rmc", factor_piece, gradient_high, preferred_element_type=jnp.float32
    )
    low_term = jnp.einsum(
        "dr,dmc->rmc", factor_piece, gradient_low, preferred_element_type=jnp.float32
    )
    partial_value = high_term + low_term
    summed = lax.psum_scatter(partial_value, "fs", scatter_dimension=0, tiled=True)
    projected = jnp.transpose(summed, (1, 0, 2))
    square_sum = lax.psum(jnp.sum(projected * projected), ("fs", "tp"))
    root_mean = jnp.sqrt(square_sum / (3 * RANK * MW) + 1e-06)
    clip_factor = jnp.minimum(1.0, 0.25 / root_mean)
    clipped = clip_factor * projected
    new_first = 0.9 * first_moment + 0.1 * clipped
    new_second = 0.95 * second_moment + 0.05 * clipped * clipped
    normed = new_first / (jnp.sqrt(new_second) + 1e-08)
    normed_whole = lax.all_gather(normed, "fs", axis=1, tiled=True)
    update = jnp.einsum("dr,mrc->mdc", factor_wide, normed_whole, precision=lax.Precision.HIGHEST)
    new_weights = weights - 0.02 * update
    copies = lax.all_gather(new_weights.astype(jnp.bfloat16), "fs", axis=1, tiled=True)
    return (update, new_weights, copies, new_first, new_second)


def solution(mesh):
    placed = (
        P("fs", None),
        P(None, "fs", "tp"),
        P("fs", None),
        P(None, "fs", "tp"),
        P(None, "fs", "tp"),
        P(None, "fs", "tp"),
    )
    return jax.shard_map(
        on_device,
        mesh=mesh,
        in_specs=placed,
        out_specs=(
            P(None, "fs", "tp"),
            P(None, "fs", "tp"),
            P(None, None, "tp"),
            P(None, "fs", "tp"),
            P(None, "fs", "tp"),
        ),
        check_vma=False,
    )
```

profile of v0, /device:TPU:0, one launch (start us, length us, event | category | flops | bytes accessed | tf_op | source)
XLA Modules:
  0.0 294.2 jit_solution(1546172498071317333)
XLA Ops:
  7.2 0.0 all-gather.3.cloned.1.call-start
  7.2 0.7 all-gather.3.cloned.1.call-update
  7.9 0.0 all-reduce.3.cloned.1.call-start
  8.0 1.1 copy-done
  9.1 10.9 %fusion = f32[2048,3,256]{2,0,1:T(8,128)} fusion(bf16[3,2048,256]{2,1,0:T(8,128)(2,1)S(1)} %copy-done, bf16[2048,2048]{1,0:T(8,128)(2,1)} %param.6), kind=kOutput, calls=%fused_computation | convolution fusion | flops 6442450944 | bytes 17825792 | tf_op jit(solution)/shard_map/td,mtc->dmc/dot_general | solution.py:12
  19.9 33.2 %all-gather.3.cloned.1.call-done = bf16[2048,256]{1,0:T(8,128)(2,1)} async-done(((bf16[256,256]{1,0:T(8,128)(2,1)}), bf16[2048,256]{1,0:T(8,128)(2,1)}) %all-gather.3.cloned.1.call-update) | async-done | bytes 1048592 | tf_op jit(solution)/shard_map/all_gather | solution.py:17
  53.2 6.0 %fusion.2 = f32[3,256,256]{2,1,0:T(8,128)S(1)} fusion(f32[2048,3,256]{2,0,1:T(8,128)} %fusion, bf16[2048,256]{1,0:T(8,128)(2,1)} %all-gather.3.cloned.1.call-done), kind=kOutput, calls=%fused_computation.3 | convolution fusion | flops 811597824 | bytes 8126464 | tf_op jit(solution)/shard_map/dr,dmc->rmc/dot_general | solution.py:21
  59.2 0.6 copy-done.1
  59.8 0.3 copy-done.2
  60.1 1.9 fusion.9
  62.0 2.4 copy.39
  64.5 0.0 all-gather.5.cloned.1.call-start
  64.5 0.6 dynamic-slice
  65.8 2.3 copy.41
  68.0 73.6 %all-reduce.3.cloned.1.call-done = f32[256,3,256]{2,1,0:T(4,128)} async-done(((f32[256,3,256]{2,1,0:T(4,128)}), f32[256,3,256]{2,1,0:T(4,128)}) %all-reduce.3.cloned.1.call-update) | async-done | bytes 786448
  141.6 1.6 multiply_reduce_fusion
  143.2 39.7 %psum.7 = f32[]{:T(128)} all-reduce(f32[]{:T(128)} %get-tuple-element.25), channel_id=1, replica_groups=mesh['fs'=8,'tp'=4] {'fs','tp'}, use_global_device_ids=true, to_apply=%region_2.0 | all-reduce | flops 1 | bytes 8 | tf_op jit(solution)/shard_map/psum | solution.py:27
  183.7 1.6 add_divide_fusion
  185.3 32.0 %all_gather.10 = f32[3,256,256]{2,1,0:T(8,128)S(1)} all-gather(f32[3,32,256]{2,1,0:T(8,128)S(1)} %get-tuple-element.22), channel_id=1, replica_groups=mesh['fs'=8,'tp'=4] {'fs'}, dimensions={1}, use_global_device_ids=true | all-gather | bytes 884736 | tf_op jit(solution)/shard_map/all_gather | solution.py:34
  217.3 3.2 %fusion.17 = (bf16[3,256,256]{1,2,0:T(8,128)(2,1)}, f32[3,256,256]{1,2,0:T(8,128)}, f32[3,256,256]{1,2,0:T(8,128)}) fusion(f32[3,256,256]{1,2,0:T(8,128)} %copy.41, f32[3,256,256]{2,1,0:T(8,128)S(1)} %all_gather.10, bf16[256,256]{1,0:T(8,128)(2,1)S(1)} %copy-done.3), kind=kOutput, calls=%fused_computation.22 | convolution fusion | flops 604569600 | bytes 3670016 | tf_op jit(solution)/shard_map/dr,mrc->mdc/dot_general | solution.py:35
  220.5 2.3 copy.42
  222.8 2.3 copy.43
  225.1 57.9 %all-gather.5.cloned.1.call-done = bf16[3,2048,256]{1,2,0:T(8,128)(2,1)} async-done(((bf16[3,256,256]{1,2,0:T(8,128)(2,1)}), bf16[3,2048,256]{1,2,0:T(8,128)(2,1)}) %all-gather.5.cloned.1.call-update) | async-done | bytes 3145744 | tf_op jit(solution)/shard_map/all_gather | solution.py:37
  283.0 4.6 %copy.44 = bf16[3,2048,256]{2,1,0:T(8,128)(2,1)} copy(bf16[3,2048,256]{1,2,0:T(8,128)(2,1)} %all-gather.5.cloned.1.call-done) | data formatting | bytes 6291456
  (11 shorter events, 0.1 us)
Async XLA Ops:
  7.2 1.9 copy-start
  7.2 46.0 %all-gather.3.cloned.1.call-start = ((), (), s32[]{:S(2)}) async-start(), calls=%async_computation | async-start | bytes 1179648 | tf_op jit(solution)/shard_map/all_gather | solution.py:17
  7.9 133.7 %all-reduce.3.cloned.1.call-start = ((), (), s32[]{:S(2)}) async-start(), calls=%async_computation.2 | async-start | bytes 2097152
  53.1 6.7 %copy-start.1 = (f32[2048,3,256]{2,0,1:T(8,128)S(1)}, f32[2048,3,256]{2,0,1:T(8,128)}, u32[]{:S(2)}) copy-start(f32[2048,3,256]{2,0,1:T(8,128)} %fusion) | copy-start | bytes 18874372
  53.2 6.9 %copy-start.2 = (bf16[2048,256]{1,0:T(8,128)(2,1)S(1)}, bf16[2048,256]{1,0:T(8,128)(2,1)}, u32[]{:S(2)}) copy-start(bf16[2048,256]{1,0:T(8,128)(2,1)} %all-gather.3.cloned.1.call-done) | copy-start | bytes 3145732
  60.1 4.4 %copy-start.5 = (u32[32]{0:T(128)S(1)}, u32[32]{0:T(128)}, u32[]{:S(2)}) copy-start(u32[32]{0:T(128)} %constant.25) | copy-start | bytes 388
  60.1 123.6 %copy-start.4 = (f32[3,32,256]{2,1,0:T(8,128)S(1)}, f32[3,32,256]{2,1,0:T(8,128)}, u32[]{:S(2)}) copy-start(f32[3,32,256]{2,1,0:T(8,128)} %param.11) | copy-start | bytes 294916
  60.1 157.2 %copy-start.3 = (bf16[256,256]{1,0:T(8,128)(2,1)S(1)}, bf16[256,256]{1,0:T(8,128)(2,1)}, u32[]{:S(2)}) copy-start(bf16[256,256]{1,0:T(8,128)(2,1)} %param.8) | copy-start | bytes 393220
  64.5 218.6 %all-gather.5.cloned.1.call-start = ((), (), s32[]{:S(2)}) async-start(), calls=%async_computation.1 | async-start | bytes 3538944 | tf_op jit(solution)/shard_map/all_gather | solution.py:37
Sparse Core Ops, SparseCore 0:
  10.1 42.9 all-gather.2
  64.6 77.0 all-reduce.2
  220.7 62.2 all-gather.4
where the time goes:
time: 295 us; the launch traced here: 294 us
  waiting for transfers between devices  165 us (56%)
  blocking collectives  71.8 us (24%)
  matrix products  22 us (7%)
  local copies, waits for them, and re-layouts  16.5 us (6%)
  between operations  15.1 us (5%)
  other arithmetic  3.21 us (1%)
    unnamed x4, waiting for transfers between devices  74.3 us
    all_gather x1, waiting for transfers between devices, on_device(): lax.all_gather(new_weights.astype(jnp.bfloat16), 'fs', axis=1, tiled=True)  57.9 us
    psum x1, blocking collectives, on_device(): square_sum = lax.psum(jnp.sum(projected * projected), ('fs', 'tp'))  39.7 us
    all_gather x1, waiting for transfers between devices, on_device(): factor_piece = lax.all_gather(factor, 'fs', axis=0, tiled=True)  33.2 us
    all_gather x1, blocking collectives, on_device(): normed_whole = lax.all_gather(normed, 'fs', axis=1, tiled=True)  32 us
    unnamed x17, local copies, waits for them, and re-layouts  14.1 us
    dot_general x1, matrix products, on_device(): jnp.einsum('td,mtc->dmc', inputs, cotangents, preferred_element_type=jnp....  10.9 us
    dot_general x1, matrix products, on_device(): jnp.einsum('dr,dmc->rmc', factor_piece, gradient_low, preferred_element_t...  6.04 us
  transfers between devices with their start and end apart: 3, of which 3 were waited for; matrix products, arithmetic and copies ran while one was open for 6% of the time, Pallas kernels for 0%

commit v1 on v0

--- a/solution.py
+++ b/solution.py
@@ -31,8 +31,22 @@
     new_first = 0.9 * first_moment + 0.1 * clipped
     new_second = 0.95 * second_moment + 0.05 * clipped * clipped
     normed = new_first / (jnp.sqrt(new_second) + 1e-08)
-    normed_whole = lax.all_gather(normed, "fs", axis=1, tiled=True)
-    update = jnp.einsum("dr,mrc->mdc", factor_wide, normed_whole, precision=lax.Precision.HIGHEST)
+    size, index, width = (lax.axis_size("fs"), lax.axis_index("fs"), normed.shape[1])
+    right = [(i, (i + 1) % size) for i in range(size)]
+    carried, running = (normed, None)
+    for lap in range(size):
+        coming = lax.ppermute(carried, "fs", right) if lap < size - 1 else None
+        take_in = jnp.einsum(
+            "dr,mrc->mdc",
+            lax.dynamic_slice_in_dim(
+                factor_wide, (index - lap) % size * width, carried.shape[1], axis=1
+            ),
+            carried,
+            precision=lax.Precision.HIGHEST,
+        )
+        running = take_in if running is None else running + take_in
+        carried = coming
+    update = running
     new_weights = weights - 0.02 * update
     copies = lax.all_gather(new_weights.astype(jnp.bfloat16), "fs", axis=1, tiled=True)
     return (update, new_weights, copies, new_first, new_second)

time: 295 us -> 312 us (1.058)
  waiting for transfers between devices: 165 us -> 209 us
  blocking collectives: 71.8 us -> 39.8 us
    ppermute x0 -> x7, waiting for transfers between devices: none -> 45.7 us  [on_device(): coming = lax.ppermute(carried, 'fs', right) if lap < size - 1 else None]
    all_gather x1 -> x0, blocking collectives: 32 us -> none  [on_device(): normed_whole = lax.all_gather(normed, 'fs', axis=1, tiled=True)]
    unnamed x17 -> x19, local copies, waits for them, and re-layouts: 14.1 us -> 14.1 us
  transfers between devices with their start and end apart: 3 -> 10, of which waited for: 3 -> 10; matrix products, arithmetic and copies ran while one was open for 6% -> 7% of each run, Pallas kernels for 0% -> 0%
where the time goes in v1:
time: 312 us; the launch traced here: 311 us
  waiting for transfers between devices  209 us (67%)
  blocking collectives  39.8 us (13%)
  matrix products  24.6 us (8%)
  local copies, waits for them, and re-layouts  16.5 us (5%)
  between operations  15.4 us (5%)
  other arithmetic  3.28 us (1%)
    unnamed x4, waiting for transfers between devices  74.1 us
    all_gather x1, waiting for transfers between devices, on_device(): lax.all_gather(new_weights.astype(jnp.bfloat16), 'fs', axis=1, tiled=True)  56.3 us
    ppermute x7, waiting for transfers between devices, on_device(): coming = lax.ppermute(carried, 'fs', right) if lap < size - 1 else None  45.7 us
    psum x1, blocking collectives, on_device(): square_sum = lax.psum(jnp.sum(projected * projected), ('fs', 'tp'))  39.8 us
    all_gather x1, waiting for transfers between devices, on_device(): factor_piece = lax.all_gather(factor, 'fs', axis=0, tiled=True)  33.2 us
    unnamed x19, local copies, waits for them, and re-layouts  14.1 us
    dot_general x1, matrix products, on_device(): jnp.einsum('td,mtc->dmc', inputs, cotangents, preferred_element_type=jnp....  10.9 us
  transfers between devices with their start and end apart: 10, of which 10 were waited for; matrix products, arithmetic and copies ran while one was open for 7% of the time, Pallas kernels for 0%

profile of v1, /device:TPU:0, one launch (start us, length us, event | category | flops | bytes accessed | tf_op | source)
XLA Modules:
  0.0 311.5 jit_solution(9350921145113298345)
XLA Ops:
  8.0 1.1 copy-done
  9.1 10.9 %fusion = f32[2048,3,256]{2,0,1:T(8,128)} fusion(bf16[3,2048,256]{2,1,0:T(8,128)(2,1)S(1)} %copy-done, bf16[2048,2048]{1,0:T(8,128)(2,1)} %param.6), kind=kOutput, calls=%fused_computation | convolution fusion | flops 6442450944 | bytes 17825792 | tf_op jit(solution)/shard_map/td,mtc->dmc/dot_general | solution.py:12
  20.0 33.2 %all-gather.3.cloned.1.call-done = bf16[2048,256]{1,0:T(8,128)(2,1)} async-done(((bf16[256,256]{1,0:T(8,128)(2,1)}), bf16[2048,256]{1,0:T(8,128)(2,1)}) %all-gather.3.cloned.1.call-update) | async-done | bytes 1048592 | tf_op jit(solution)/shard_map/all_gather | solution.py:17
  53.2 6.0 %fusion.2 = f32[3,256,256]{2,1,0:T(8,128)S(1)} fusion(f32[2048,3,256]{2,0,1:T(8,128)} %fusion, bf16[2048,256]{1,0:T(8,128)(2,1)} %all-gather.3.cloned.1.call-done), kind=kOutput, calls=%fused_computation.3 | convolution fusion | flops 811597824 | bytes 8126464 | tf_op jit(solution)/shard_map/dr,dmc->rmc/dot_general | solution.py:21
  60.1 1.9 fusion.10
  62.0 2.4 copy.41
  65.9 2.3 copy.51
  68.2 73.4 %all-reduce.3.cloned.1.call-done = f32[256,3,256]{2,1,0:T(4,128)} async-done(((f32[256,3,256]{2,1,0:T(4,128)}), f32[256,3,256]{2,1,0:T(4,128)}) %all-reduce.3.cloned.1.call-update) | async-done | bytes 786448
  141.6 1.6 multiply_reduce_fusion
  143.2 39.8 %psum.7 = f32[]{:T(128)} all-reduce(f32[]{:T(128)} %get-tuple-element.20), channel_id=1, replica_groups=mesh['fs'=8,'tp'=4] {'fs','tp'}, use_global_device_ids=true, to_apply=%region_2.0 | all-reduce | flops 1 | bytes 8 | tf_op jit(solution)/shard_map/psum | solution.py:27
  183.7 1.7 add_divide_fusion
  185.4 2.5 collective-permute-start
  188.4 4.3 %collective-permute-done = f32[3,32,256]{2,1,0:T(8,128)S(1)} collective-permute-done((f32[3,32,256]{2,1,0:T(8,128)S(1)}, f32[3,32,256]{2,1,0:T(8,128)S(1)}, u32[]{:S(2)}, u32[]{:S(2)}) %collective-permute-start) | collective-permute-done | bytes 98336 | tf_op jit(solution)/shard_map/ppermute | solution.py:38
  193.3 6.7 %collective-permute-done.1 = f32[3,32,256]{2,1,0:T(8,128)S(1)} collective-permute-done((f32[3,32,256]{2,1,0:T(8,128)S(1)}, f32[3,32,256]{2,1,0:T(8,128)S(1)}, u32[]{:S(2)}, u32[]{:S(2)}) %collective-permute-start.1) | collective-permute-done | bytes 98336 | tf_op jit(solution)/shard_map/ppermute | solution.py:38
  200.6 6.7 %collective-permute-done.2 = f32[3,32,256]{2,1,0:T(8,128)S(1)} collective-permute-done((f32[3,32,256]{2,1,0:T(8,128)S(1)}, f32[3,32,256]{2,1,0:T(8,128)S(1)}, u32[]{:S(2)}, u32[]{:S(2)}) %collective-permute-start.2) | collective-permute-done | bytes 98336 | tf_op jit(solution)/shard_map/ppermute | solution.py:38
  207.9 6.8 %collective-permute-done.3 = f32[3,32,256]{2,1,0:T(8,128)S(1)} collective-permute-done((f32[3,32,256]{2,1,0:T(8,128)S(1)}, f32[3,32,256]{2,1,0:T(8,128)S(1)}, u32[]{:S(2)}, u32[]{:S(2)}) %collective-permute-start.3) | collective-permute-done | bytes 98336 | tf_op jit(solution)/shard_map/ppermute | solution.py:38
  215.3 7.6 %collective-permute-done.4 = f32[3,32,256]{2,1,0:T(8,128)S(1)} collective-permute-done((f32[3,32,256]{2,1,0:T(8,128)S(1)}, f32[3,32,256]{2,1,0:T(8,128)S(1)}, u32[]{:S(2)}, u32[]{:S(2)}) %collective-permute-start.4) | collective-permute-done | bytes 98336 | tf_op jit(solution)/shard_map/ppermute | solution.py:38
  223.5 6.8 %collective-permute-done.5 = f32[3,32,256]{2,1,0:T(8,128)S(1)} collective-permute-done((f32[3,32,256]{2,1,0:T(8,128)S(1)}, f32[3,32,256]{2,1,0:T(8,128)S(1)}, u32[]{:S(2)}, u32[]{:S(2)}) %collective-permute-start.5) | collective-permute-done | bytes 98336 | tf_op jit(solution)/shard_map/ppermute | solution.py:38
  230.8 6.7 %collective-permute-done.6 = f32[3,32,256]{2,1,0:T(8,128)S(1)} collective-permute-done((f32[3,32,256]{2,1,0:T(8,128)S(1)}, f32[3,32,256]{2,1,0:T(8,128)S(1)}, u32[]{:S(2)}, u32[]{:S(2)}) %collective-permute-start.6) | collective-permute-done | bytes 98336 | tf_op jit(solution)/shard_map/ppermute | solution.py:38
  237.5 1.8 fusion.42
  239.4 2.3 copy.52
  241.7 2.3 copy.53
  244.0 56.3 %all-gather.5.cloned.1.call-done = bf16[3,2048,256]{1,2,0:T(8,128)(2,1)} async-done(((bf16[3,256,256]{1,2,0:T(8,128)(2,1)}), bf16[3,2048,256]{1,2,0:T(8,128)(2,1)}) %all-gather.5.cloned.1.call-update) | async-done | bytes 3145744 | tf_op jit(solution)/shard_map/all_gather | solution.py:51
  300.3 4.6 %copy.54 = bf16[3,2048,256]{2,1,0:T(8,128)(2,1)} copy(bf16[3,2048,256]{1,2,0:T(8,128)(2,1)} %all-gather.5.cloned.1.call-done) | data formatting | bytes 6291456
  (33 shorter events, 6.3 us)
Async XLA Ops:
  7.2 1.9 copy-start
  7.2 46.0 %all-gather.3.cloned.1.call-start = ((), (), s32[]{:S(2)}) async-start(), calls=%async_computation | async-start | bytes 1179648 | tf_op jit(solution)/shard_map/all_gather | solution.py:17
  7.9 133.7 %all-reduce.3.cloned.1.call-start = ((), (), s32[]{:S(2)}) async-start(), calls=%async_computation.2 | async-start | bytes 2097152
  53.1 6.7 %copy-start.1 = (f32[2048,3,256]{2,0,1:T(8,128)S(1)}, f32[2048,3,256]{2,0,1:T(8,128)}, u32[]{:S(2)}) copy-start(f32[2048,3,256]{2,0,1:T(8,128)} %fusion) | copy-start | bytes 18874372
  53.2 6.9 %copy-start.4 = (bf16[2048,256]{1,0:T(8,128)(2,1)S(1)}, bf16[2048,256]{1,0:T(8,128)(2,1)}, u32[]{:S(2)}) copy-start(bf16[2048,256]{1,0:T(8,128)(2,1)} %all-gather.3.cloned.1.call-done) | copy-start | bytes 3145732
  60.1 4.6 %copy-start.6 = (u32[32]{0:T(128)S(1)}, u32[32]{0:T(128)}, u32[]{:S(2)}) copy-start(u32[32]{0:T(128)} %constant.98) | copy-start | bytes 388
  60.1 123.6 %copy-start.5 = (f32[3,32,256]{2,1,0:T(8,128)S(1)}, f32[3,32,256]{2,1,0:T(8,128)}, u32[]{:S(2)}) copy-start(f32[3,32,256]{2,1,0:T(8,128)} %param.11) | copy-start | bytes 294916
  60.1 127.7 %copy-start.2 = (bf16[256,256]{1,0:T(8,128)(2,1)S(1)}, bf16[256,256]{1,0:T(8,128)(2,1)}, u32[]{:S(2)}) copy-start(bf16[256,256]{1,0:T(8,128)(2,1)} %param.8) | copy-start | bytes 393220
  64.5 235.8 %all-gather.5.cloned.1.call-start = ((), (), s32[]{:S(2)}) async-start(), calls=%async_computation.1 | async-start | bytes 3538944 | tf_op jit(solution)/shard_map/all_gather | solution.py:51
  183.7 53.9 %copy-start.3 = (f32[3,256,256]{1,2,0:T(8,128)S(1)}, f32[3,256,256]{1,2,0:T(8,128)}, u32[]{:S(2)}) copy-start(f32[3,256,256]{1,2,0:T(8,128)} %copy.51) | copy-start | bytes 2359300
  185.4 7.3 %collective-permute-start = (f32[3,32,256]{2,1,0:T(8,128)S(1)}, f32[3,32,256]{2,1,0:T(8,128)S(1)}, u32[]{:S(2)}, u32[]{:S(2)}) collective-permute-start(f32[3,32,256]{2,1,0:T(8,128)S(1)} %get-tuple-element.17), channel_id=1, source_target_pairs={{0,4},{4,8},{8,12},{12,16},{16,20},{20,24},{24,28},{28,0},{1,5},{5... | collective-permute-start | bytes 294920 | tf_op jit(solution)/shard_map/ppermute | solution.py:38
  192.7 7.3 %collective-permute-start.1 = (f32[3,32,256]{2,1,0:T(8,128)S(1)}, f32[3,32,256]{2,1,0:T(8,128)S(1)}, u32[]{:S(2)}, u32[]{:S(2)}) collective-permute-start(f32[3,32,256]{2,1,0:T(8,128)S(1)} %collective-permute-done), channel_id=1, source_target_pairs={{0,4},{4,8},{8,12},{12,16},{16,20},{20,24},{24,28},{28,0},{1,5},{5... | collective-permute-start | bytes 294920 | tf_op jit(solution)/shard_map/ppermute | solution.py:38
  200.0 7.3 %collective-permute-start.2 = (f32[3,32,256]{2,1,0:T(8,128)S(1)}, f32[3,32,256]{2,1,0:T(8,128)S(1)}, u32[]{:S(2)}, u32[]{:S(2)}) collective-permute-start(f32[3,32,256]{2,1,0:T(8,128)S(1)} %collective-permute-done.1), channel_id=1, source_target_pairs={{0,4},{4,8},{8,12},{12,16},{16,20},{20,24},{24,28},{28,0},{1,5},{5... | collective-permute-start | bytes 294920 | tf_op jit(solution)/shard_map/ppermute | solution.py:38
  207.3 7.4 %collective-permute-start.3 = (f32[3,32,256]{2,1,0:T(8,128)S(1)}, f32[3,32,256]{2,1,0:T(8,128)S(1)}, u32[]{:S(2)}, u32[]{:S(2)}) collective-permute-start(f32[3,32,256]{2,1,0:T(8,128)S(1)} %collective-permute-done.2), channel_id=1, source_target_pairs={{0,4},{4,8},{8,12},{12,16},{16,20},{20,24},{24,28},{28,0},{1,5},{5... | collective-permute-start | bytes 294920 | tf_op jit(solution)/shard_map/ppermute | solution.py:38
  214.7 8.2 %collective-permute-start.4 = (f32[3,32,256]{2,1,0:T(8,128)S(1)}, f32[3,32,256]{2,1,0:T(8,128)S(1)}, u32[]{:S(2)}, u32[]{:S(2)}) collective-permute-start(f32[3,32,256]{2,1,0:T(8,128)S(1)} %collective-permute-done.3), channel_id=1, source_target_pairs={{0,4},{4,8},{8,12},{12,16},{16,20},{20,24},{24,28},{28,0},{1,5},{5... | collective-permute-start | bytes 294920 | tf_op jit(solution)/shard_map/ppermute | solution.py:38
  222.9 7.3 %collective-permute-start.5 = (f32[3,32,256]{2,1,0:T(8,128)S(1)}, f32[3,32,256]{2,1,0:T(8,128)S(1)}, u32[]{:S(2)}, u32[]{:S(2)}) collective-permute-start(f32[3,32,256]{2,1,0:T(8,128)S(1)} %collective-permute-done.4), channel_id=1, source_target_pairs={{0,4},{4,8},{8,12},{12,16},{16,20},{20,24},{24,28},{28,0},{1,5},{5... | collective-permute-start | bytes 294920 | tf_op jit(solution)/shard_map/ppermute | solution.py:38
  230.2 7.3 %collective-permute-start.6 = (f32[3,32,256]{2,1,0:T(8,128)S(1)}, f32[3,32,256]{2,1,0:T(8,128)S(1)}, u32[]{:S(2)}, u32[]{:S(2)}) collective-permute-start(f32[3,32,256]{2,1,0:T(8,128)S(1)} %collective-permute-done.5), channel_id=1, source_target_pairs={{0,4},{4,8},{8,12},{12,16},{16,20},{20,24},{24,28},{28,0},{1,5},{5... | collective-permute-start | bytes 294920 | tf_op jit(solution)/shard_map/ppermute | solution.py:38
Sparse Core Ops, SparseCore 0:
  10.1 42.9 all-gather.2
  64.6 77.0 all-reduce.2
  239.5 60.7 all-gather.4
